TPU v7x, 32 devices: a whole 2x2x4 slice. The times are simulated.
32 devices in a mesh: rep: 4 (over z), fs: 4 (over y, x), tp: 2 (over core).
Axes of the slice: x: 2, y: 2, z: 4, core: 2. Of those that a mesh axis runs over, the one named last changes fastest.
Arguments:
- inputs: bfloat16 [4096, 2048], P(('rep', 'fs', 'tp')), may hold values from -6 to 6
- out_grad: bfloat16 [4096, 2048], P(('rep', 'fs', 'tp')), may hold values from -6 to 6
- pre_act: bfloat16 [4096, 8192], P('rep', ('fs', 'tp')), may hold values from -6 to 6
- w_up: bfloat16 [2048, 8192], P('rep', ('fs', 'tp')), may hold values from -0.125 to 0.125
- w_down_t: bfloat16 [2048, 8192], P('rep', ('fs', 'tp')), may hold values from -0.0625 to 0.0625
Outputs:
- grad_in: bfloat16 [4096, 2048], P(('rep', 'fs', 'tp'))
- grad_up: float32 [2048, 8192], P('rep', ('fs', 'tp'))
- grad_down_t: float32 [2048, 8192], P('rep', ('fs', 'tp'))
All inputs are finite; a program needn't handle non-finite values.
Results may differ from a plain program's by a relative error of at most 0.014.
Values may be sent and summed in bfloat16 or wider, within the bound.
A program may use at most 128 MiB of HBM per device.

v0:
```python
import functools

import jax
import jax.numpy as jnp
from jax import lax
from jax.experimental import pallas as pl
from jax.experimental.pallas import tpu as pltpu
from jax.sharding import PartitionSpec as P

BF16 = jnp.bfloat16
F32 = jnp.float32


def kernel(
    n, n_fs, chunks, factor,
    x_ref, og_ref, pre_ref, wu_ref, wd_ref,
    gin_ref, gu_ref, gd_ref,
    x_all, og_all, wu_all, wd_all, sq, gp, rs, tbuf, prec, frec,
    pre, total, zs, zr, xs, xr, cs, cr, ts, tr, fsend, frecv, ls,
):
    r, f, t = lax.axis_index("rep"), lax.axis_index("fs"), lax.axis_index("tp")
    tok, d_model = og_ref.shape
    shard, cols = wd_ref.shape
    crow = shard // chunks
    partner = {"tp": 1 - t}
    own_tokens = pl.ds(pl.multiple_of((f * 2 + t) * tok, tok), tok)
    loads = [
        pltpu.make_async_copy(src, dst, ls.at[i])
        for i, (src, dst) in enumerate((
            (pre_ref, pre),
            (og_ref, og_all.at[own_tokens, :]),
            (x_ref, x_all.at[own_tokens, :]),
            (wd_ref, wd_all.at[r]),
            (wu_ref, wu_all.at[r]),
        ))
    ]
    peers = [None] + [{"fs": lax.rem(f + d, n_fs)} for d in range(1, n_fs)]
    ahead = ({"rep": lax.rem(r + 1, n)}, {"rep": lax.rem(r + n - 1, n)})
    depth = (r, n - 1 - r)
    has_prev = (r > 0, r < n - 1)
    has_next = (r < n - 1, r > 0)

    barrier = pltpu.get_barrier_semaphore()
    for way in range(2):
        @pl.when(has_next[way])
        def _(way=way):
            pl.semaphore_signal(barrier, inc=1, device_id=ahead[way])
    for d in range(1, n_fs):
        pl.semaphore_signal(barrier, inc=1, device_id=peers[d])
    pl.semaphore_signal(barrier, inc=1, device_id=partner)
    pl.semaphore_wait(
        barrier, n_fs + jnp.where(r > 0, 1, 0) + jnp.where(r < n - 1, 1, 0)
    )

    def remote(src, dst, send, recv, target):
        return pltpu.make_async_remote_copy(
            src_ref=src, dst_ref=dst, send_sem=send, recv_sem=recv,
            device_id=target, device_id_type=pl.DeviceIdType.MESH,
        )

    def rows_of(ref, ff, tt):
        return ref.at[pl.ds(pl.multiple_of((ff * 2 + tt) * tok, tok), tok), :]

    def z_copy(phase, way, k, j, src, dst):
        return remote(
            src, dst, zs.at[phase, way, k, j], zr.at[phase, way, k, j], ahead[way]
        )

    def piece(ref, j):
        return ref.at[pl.ds(pl.multiple_of(j * crow, crow), crow), :]

    def send_own(phase, own, everyone, when):
        for way in range(2):
            @pl.when(jnp.logical_and(has_next[way], when[way]))
            def _(way=way):
                for j in range(chunks):
                    z_copy(
                        phase, way, 0, j, piece(own, j), piece(everyone.at[r], j)
                    ).start()

    def spread_start(q, own, everyone):
        for d in range(1, n_fs):
            remote(
                own, rows_of(everyone, f, t), xs.at[q, d], xr.at[q, d], peers[d]
            ).start()
        remote(
            own, rows_of(everyone, f, t), cs.at[q, 0], cr.at[q, 0], partner
        ).start()

    def spread_pass(q, everyone):
        for d in range(1, n_fs):
            src = rows_of(everyone, lax.rem(f + n_fs - d, n_fs), t)
            remote(src, src, xs.at[q, d], xr.at[q, d], peers[d]).wait()
            remote(src, src, cs.at[q, d], cr.at[q, d], partner).start()

    def spread_end(q, everyone):
        for d in range(n_fs):
            there = rows_of(everyone, lax.rem(f + n_fs - d, n_fs), 1 - t)
            remote(there, there, cs.at[q, d], cr.at[q, d], partner).wait()

    send_own(0, wd_ref, wd_all, (True, True))
    spread_start(0, og_ref, og_all)
    send_own(1, wu_ref, wu_all, (depth[0] == 0, depth[1] == 0))
    for load in loads:
        load.start()
    for load in loads:
        load.wait()
    tile = 2 * tok

    def square(i, _):
        at = pl.ds(pl.multiple_of(i * tile, tile), tile)
        linear = jnp.maximum(pre[at, :].astype(F32), 0.0)
        sq[at, :] = (linear * linear).astype(BF16)
        return 0

    lax.fori_loop(0, n_fs, square, 0)
    spread_pass(0, og_all)
    spread_end(0, og_all)
    spread_start(1, x_ref, x_all)

    def partial(left, right, s, j):
        at = pl.ds(pl.multiple_of(s * shard + j * crow, crow), crow)
        return lax.dot_general(
            left[:, at], right[...], (((0,), (0,)), ((), ())),
            preferred_element_type=F32,
        ) * factor

    def one_round(phase, everyone, left, right, k):
        def one_piece(j, _):
            at = pl.ds(pl.multiple_of(j * crow, crow), crow)
            for way in range(2):
                sign = 1 - 2 * way
                slots = rs.at[phase, way]

                @pl.when(k < depth[way])
                def _(way=way, sign=sign):
                    block = piece(everyone.at[r - sign * (1 + k)], j)
                    z_copy(phase, way, k, j, block, block).wait_recv()

                    @pl.when(has_next[way])
                    def _():
                        z_copy(phase, way, k + 1, j, block, block).start()

                @pl.when(k >= depth[way])
                def _(way=way, slots=slots):
                    back = k - depth[way]
                    s = n - 1 - back if way == 0 else back
                    term = partial(left, right, s, j)
                    block = piece(slots.at[s], j)

                    @pl.when(has_prev[way])
                    def _():
                        z_copy(phase, way, k, j, block, block).wait_recv()
                        slots[s, at, :] = (term + slots[s, at, :].astype(F32)).astype(BF16)

                    @pl.when(jnp.logical_not(has_prev[way]))
                    def _():
                        slots[s, at, :] = term.astype(BF16)

                    z_copy(phase, way, k + 1, j, block, block).start()
            return 0

        lax.fori_loop(0, chunks, one_piece, 0)

    def last_round(phase, left, right, out, low, high):
        def one_piece(j, _):
            at = pl.ds(pl.multiple_of(j * crow, crow), crow)
            total[...] = partial(left, right, r, j)
            for way in range(2):
                @pl.when(has_prev[way])
                def _(way=way):
                    block = piece(rs.at[phase, way, r], j)
                    z_copy(phase, way, n - 1, j, block, block).wait_recv()
                    total[...] += rs[phase, way, r, at, :].astype(F32)
            out[at, :] = total[...].astype(BF16)
            return 0

        lax.fori_loop(low, high, one_piece, 0)

    def round_down(k, _):
        one_round(0, wd_all, og_all, sq, k)
        send_own(1, wu_ref, wu_all, (depth[0] == k + 1, depth[1] == k + 1))
        return 0

    lax.fori_loop(0, n - 1, round_down, 0)
    spread_pass(1, x_all)

    def make_grad_pre(i, _):
        at = pl.ds(pl.multiple_of(i * tile, tile), tile)
        acc = jnp.zeros((tile, cols), F32)
        for s in range(n):
            acc += jnp.dot(
                og_all[at, s * shard:(s + 1) * shard], wd_all[s],
                preferred_element_type=F32,
            )
        linear = jnp.maximum(pre[at, :].astype(F32), 0.0)
        gp[at, :] = (acc * 2.0 * linear).astype(BF16)
        return 0

    lax.fori_loop(0, n_fs, make_grad_pre, 0)
    spread_end(1, x_all)

    def cross(s):
        return remote(tbuf.at[s, 1 - t], prec.at[s], ts.at[s], tr.at[s], partner)

    def out_copy(s, d):
        rows = pl.ds(pl.multiple_of(lax.rem(f + d, n_fs) * tok, tok), tok)
        return remote(
            prec.at[s, rows, :], frec.at[s, d - 1],
            fsend.at[s, d], frecv.at[s, d], peers[d],
        )

    def block_term(s):
        def body(i, _):
            at = pl.ds(pl.multiple_of(i * tile, tile), tile)
            here = pl.ds(pl.multiple_of(i * tok, tok), tok)
            term = lax.dot_general(
                gp[at, :], wu_all[s], (((1,), (1,)), ((), ())),
                preferred_element_type=F32,
            ).astype(BF16)
            tbuf[s, 0, here, :] = term[:tok]
            tbuf[s, 1, here, :] = term[tok:]
            return 0

        lax.fori_loop(0, n_fs, body, 0)
        cross(s).start()

    def chip_sum(s):
        cross(s).wait()

        def body(i, _):
            here = pl.ds(pl.multiple_of(i * tok, tok), tok)
            prec[s, here, :] = (
                prec[s, here, :].astype(F32) + tbuf[s, t, here, :].astype(F32)
            ).astype(BF16)
            return 0

        lax.fori_loop(0, n_fs, body, 0)
        for d in range(1, n_fs):
            out_copy(s, d).start()

    def for_new(k, work):
        def body(way, _):
            @pl.when(jnp.where(way == 0, k < r, k < n - 1 - r))
            def _():
                work(jnp.where(way == 0, r - 1 - k, r + 1 + k))
            return 0

        lax.fori_loop(0, 2, body, 0)

    one_round(1, wu_all, x_all, gp, 0)
    block_term(r)
    for_new(0, block_term)
    last_round(0, og_all, sq, gd_ref, 0, chunks)
    chip_sum(r)

    def round_up(k, _):
        one_round(1, wu_all, x_all, gp, k)
        for_new(k, block_term)
        for_new(k - 1, chip_sum)
        return 0

    lax.fori_loop(1, n - 1, round_up, 0)
    for_new(n - 2, chip_sum)
    last_round(1, x_all, gp, gu_ref, 0, chunks - 1)

    own_rows = pl.ds(pl.multiple_of(f * tok, tok), tok)
    for s in range(n):
        acc = prec[s, own_rows, :].astype(F32)
        for d in range(1, n_fs):
            out_copy(s, d).wait()
            acc += frec[s, d - 1].astype(F32)
        gin_ref[:, s * shard:(s + 1) * shard] = acc.astype(BF16)
    last_round(1, x_all, gp, gu_ref, chunks - 1, chunks)

    for way in range(2):
        @pl.when(has_next[way])
        def _(way=way):
            def body(k, _):
                for phase in range(2):
                    for j in range(chunks):
                        block = piece(rs.at[0, 0, 0], j)
                        z_copy(phase, way, k, j, block, block).wait_send()
                return 0

            lax.fori_loop(0, n, body, 0)


def on_device(n, n_fs, inputs, out_grad, pre_act, w_up, w_down_t):
    tok, d_model = inputs.shape
    group, cols = pre_act.shape
    shard = w_up.shape[0]
    chunks = max(1, shard // 128)
    factor = float(group * n) ** -0.5
    dma = pltpu.SemaphoreType.DMA
    vmem = pl.BlockSpec(memory_space=pltpu.VMEM)
    grad_in, grad_up, grad_down_t = pl.pallas_call(
        functools.partial(kernel, n, n_fs, chunks, factor),
        out_shape=(
            jax.ShapeDtypeStruct((tok, d_model), BF16),
            jax.ShapeDtypeStruct((shard, cols), BF16),
            jax.ShapeDtypeStruct((shard, cols), BF16),
        ),
        in_specs=[pl.BlockSpec(memory_space=pl.ANY)] * 5,
        out_specs=(vmem,) * 3,
        scratch_shapes=[
            pltpu.VMEM((group, d_model), BF16),
            pltpu.VMEM((group, d_model), BF16),
            pltpu.VMEM((n, shard, cols), BF16),
            pltpu.VMEM((n, shard, cols), BF16),
            pltpu.VMEM((group, cols), BF16),
            pltpu.VMEM((group, cols), BF16),
            pltpu.VMEM((2, 2, n, shard, cols), BF16),
            pltpu.VMEM((n, 2, n_fs * tok, shard), BF16),
            pltpu.VMEM((n, n_fs * tok, shard), BF16),
            pltpu.VMEM((n, n_fs - 1, tok, shard), BF16),
            pltpu.VMEM((group, cols), BF16),
            pltpu.VMEM((shard // chunks, cols), F32),
            dma((2, 2, n, chunks)),
            dma((2, 2, n, chunks)),
            dma((2, n_fs)),
            dma((2, n_fs)),
            dma((2, n_fs)),
            dma((2, n_fs)),
            dma((n,)),
            dma((n,)),
            dma((n, n_fs)),
            dma((n, n_fs)),
            dma((5,)),
        ],
        compiler_params=pltpu.CompilerParams(
            collective_id=0, has_side_effects=True, vmem_limit_bytes=67043328
        ),
    )(inputs, out_grad, pre_act, w_up, w_down_t)
    return grad_in, grad_up.astype(F32), grad_down_t.astype(F32)


def solution(mesh):
    rows = P(("rep", "fs", "tp"), None)
    blocks = P("rep", ("fs", "tp"))
    return jax.shard_map(
        functools.partial(on_device, mesh.shape["rep"], mesh.shape["fs"]),
        mesh=mesh,
        in_specs=(rows, rows, blocks, blocks, blocks),
        out_specs=(rows, blocks, blocks),
        check_vma=False,
    )
```

profile of v0, /device:TPU:0, one launch (start us, length us, event | category | flops | bytes accessed | tf_op | source)
XLA Modules:
  0.0 201.3 jit_solution(9214245214395969893)
XLA Ops:
  0.6 195.4 %shard_map.76 = (bf16[128,2048]{1,0:T(8,128)(2,1)}, bf16[512,1024]{1,0:T(8,128)(2,1)}, bf16[512,1024]{1,0:T(8,128)(2,1)}) custom-call(bf16[128,2048]{1,0:T(8,128)(2,1)} %x_ref.1, bf16[128,2048]{1,0:T(8,128)(2,1)} %og_ref.1, bf16[1024,1024]{1,0:T(8,128)(2,1)} %pre_ref.1, bf16[512,1024]{1,0:T(8,128)(2,1)} %wu_ref.1, bf16[512,1024]{1,0:T(8,128)(2,1)} %wd_ref.1), custom_call_target="tpu_custom_call" | custom-call | tf_op jit(solution)/shard_map/pallas_call | solution.py:297
  196.0 0.0 copy-start
  196.0 2.9 %convert_element_type.6 = f32[512,1024]{1,0:T(8,128)} convert(bf16[512,1024]{1,0:T(8,128)(2,1)} %get-tuple-element.7) | non-fusion elementwise | flops 524288 | bytes 3145728 | tf_op jit(solution)/shard_map/convert_element_type | solution.py:335
  198.9 0.0 copy-done
  198.9 0.0 copy-start.1
  198.9 1.6 convert_element_type.7
  200.5 0.0 copy-done.1
  200.5 0.8 copy.9
Async XLA Ops:
  196.0 2.9 %copy-start = (bf16[512,1024]{1,0:T(8,128)(2,1)S(1)}, bf16[512,1024]{1,0:T(8,128)(2,1)}, u32[]{:S(2)}) copy-start(bf16[512,1024]{1,0:T(8,128)(2,1)} %get-tuple-element.8) | copy-start | bytes 3145732
  198.9 1.6 copy-start.1
where the time goes:
time: 201 us
  Pallas kernels  195 us (97%)
  other arithmetic  4.44 us (2%)
    pallas_call x1, Pallas kernels, on_device(): pl.pallas_call(functools.partial(kernel, n, n_fs, chunks, factor), out_sh...  195 us
    convert_element_type x2, other arithmetic, on_device(): return (grad_in, grad_up.astype(F32), grad_down_t.astype(F32))  4.44 us

commit v1 on v0

v1 whole, which is shorter than its diff:
```python
import functools

import jax
import jax.numpy as jnp
from jax import lax
from jax.experimental import pallas as pl
from jax.experimental.pallas import tpu as pltpu
from jax.sharding import PartitionSpec as P

BF16 = jnp.bfloat16
F32 = jnp.float32


def kernel(
    n, n_fs, chunks, factor,
    x_ref, og_ref, pre_ref, wu_ref, wd_ref,
    gin_ref, gu_ref, gd_ref,
    rows_all, w_all, act, rs, tbuf, prec, frec, pre, total,
    zs, zr, xs, xr, cs, cr, ts, tr, fsend, frecv, ls,
):
    r, f, t = lax.axis_index("rep"), lax.axis_index("fs"), lax.axis_index("tp")
    tok, d_model = og_ref.shape
    shard, cols = wd_ref.shape
    crow = shard // chunks
    partner = {"tp": 1 - t}
    own_tokens = pl.ds(pl.multiple_of((f * 2 + t) * tok, tok), tok)
    own_rows_of = (og_ref, x_ref)
    own_w = (wd_ref, wu_ref)
    loads = [
        pltpu.make_async_copy(src, dst, ls.at[i])
        for i, (src, dst) in enumerate((
            (pre_ref, pre),
            (og_ref, rows_all.at[0, own_tokens, :]),
            (x_ref, rows_all.at[1, own_tokens, :]),
            (wd_ref, w_all.at[0, r]),
            (wu_ref, w_all.at[1, r]),
        ))
    ]
    peers = [None] + [{"fs": lax.rem(f + d, n_fs)} for d in range(1, n_fs)]
    ahead = ({"rep": lax.rem(r + 1, n)}, {"rep": lax.rem(r + n - 1, n)})
    depth = (r, n - 1 - r)
    after = (n - 1 - r, r)
    has_next = (r < n - 1, r > 0)

    barrier = pltpu.get_barrier_semaphore()
    for way in range(2):
        @pl.when(has_next[way])
        def _(way=way):
            pl.semaphore_signal(barrier, inc=1, device_id=ahead[way])
    for d in range(1, n_fs):
        pl.semaphore_signal(barrier, inc=1, device_id=peers[d])
    pl.semaphore_signal(barrier, inc=1, device_id=partner)
    pl.semaphore_wait(
        barrier, n_fs + jnp.where(r > 0, 1, 0) + jnp.where(r < n - 1, 1, 0)
    )

    def remote(src, dst, send, recv, target):
        return pltpu.make_async_remote_copy(
            src_ref=src, dst_ref=dst, send_sem=send, recv_sem=recv,
            device_id=target, device_id_type=pl.DeviceIdType.MESH,
        )

    def rows_of(q, ff, tt):
        return rows_all.at[
            q, pl.ds(pl.multiple_of((ff * 2 + tt) * tok, tok), tok), :
        ]

    def z_copy(p, way, k, j, src, dst):
        return remote(
            src, dst, zs.at[p, way, k, j], zr.at[p, way, k, j], ahead[way]
        )

    def rows_at(j):
        return pl.ds(pl.multiple_of(j * crow, crow), crow)

    def send_own(p, way):
        for j in range(chunks):
            z_copy(
                p, way, 0, j,
                own_w[p].at[rows_at(j), :], w_all.at[p, r, rows_at(j), :],
            ).start()

    def spread_start(q):
        own = own_rows_of[q]
        for d in range(1, n_fs):
            remote(
                own, rows_of(q, f, t), xs.at[q, d], xr.at[q, d], peers[d]
            ).start()
        remote(own, rows_of(q, f, t), cs.at[q, 0], cr.at[q, 0], partner).start()

    def spread_pass(q):
        for d in range(1, n_fs):
            src = rows_of(q, lax.rem(f + n_fs - d, n_fs), t)
            remote(src, src, xs.at[q, d], xr.at[q, d], peers[d]).wait()
            remote(src, src, cs.at[q, d], cr.at[q, d], partner).start()

    def spread_end(q):
        for d in range(n_fs):
            there = rows_of(q, lax.rem(f + n_fs - d, n_fs), 1 - t)
            remote(there, there, cs.at[q, d], cr.at[q, d], partner).wait()

    for way in range(2):
        @pl.when(has_next[way])
        def _(way=way):
            send_own(0, way)
    spread_start(0)
    for way in range(2):
        @pl.when(depth[way] == 0)
        def _(way=way):
            send_own(1, way)
    for load in loads:
        load.start()
    for load in loads:
        load.wait()
    tile = 2 * tok

    def square(i, _):
        at = pl.ds(pl.multiple_of(i * tile, tile), tile)
        linear = jnp.maximum(pre[at, :].astype(F32), 0.0)
        act[0, at, :] = (linear * linear).astype(BF16)
        return 0

    lax.fori_loop(0, n_fs, square, 0)

    def partial(p, s, j):
        at = pl.ds(pl.multiple_of(s * shard + j * crow, crow), crow)
        return lax.dot_general(
            rows_all[p, :, at], act[p], (((0,), (0,)), ((), ())),
            preferred_element_type=F32,
        ) * factor

    def own_partial(p):
        def body(j, _):
            total[p, rows_at(j), :] = partial(p, r, j)
            return 0

        lax.fori_loop(0, chunks, body, 0)

    def make_grad_pre(i, _):
        at = pl.ds(pl.multiple_of(i * tile, tile), tile)
        acc = jnp.zeros((tile, cols), F32)
        for s in range(n):
            acc += jnp.dot(
                rows_all[0, at, s * shard:(s + 1) * shard], w_all[0, s],
                preferred_element_type=F32,
            )
        linear = jnp.maximum(pre[at, :].astype(F32), 0.0)
        act[1, at, :] = (acc * 2.0 * linear).astype(BF16)
        return 0

    def cross(s):
        return remote(tbuf.at[s, 1 - t], prec.at[s], ts.at[s], tr.at[s], partner)

    def out_copy(s, d):
        rows = pl.ds(pl.multiple_of(lax.rem(f + d, n_fs) * tok, tok), tok)
        return remote(
            prec.at[s, rows, :], frec.at[s, d - 1],
            fsend.at[s, d], frecv.at[s, d], peers[d],
        )

    def block_term(s):
        def body(i, _):
            at = pl.ds(pl.multiple_of(i * tile, tile), tile)
            here = pl.ds(pl.multiple_of(i * tok, tok), tok)
            term = lax.dot_general(
                act[1, at, :], w_all[1, s], (((1,), (1,)), ((), ())),
                preferred_element_type=F32,
            ).astype(BF16)
            tbuf[s, 0, here, :] = term[:tok]
            tbuf[s, 1, here, :] = term[tok:]
            return 0

        lax.fori_loop(0, n_fs, body, 0)
        cross(s).start()

    def chip_sum(s):
        cross(s).wait()

        def body(i, _):
            here = pl.ds(pl.multiple_of(i * tok, tok), tok)
            prec[s, here, :] = (
                prec[s, here, :].astype(F32) + tbuf[s, t, here, :].astype(F32)
            ).astype(BF16)
            return 0

        lax.fori_loop(0, n_fs, body, 0)
        for d in range(1, n_fs):
            out_copy(s, d).start()

    def arrivals(step, way, j):
        d, h = depth[way], after[way]
        sign = 1 - 2 * way
        ag = step <= 2 * d
        p_ag = jnp.where(step > d, 1, 0)
        k = step - 1 - p_ag * d
        q = step - 2 * d - 1
        p_rs = jnp.where(q > h, 1, 0)
        i = q - p_rs * (h + 1) - jnp.where((d == 0) & (p_rs == 0), 1, 0)

        @pl.when(ag)
        def _():
            block = w_all.at[p_ag, r - sign * (1 + k), rows_at(j), :]
            z_copy(p_ag, way, k, j, block, block).wait_recv()

            @pl.when(h > 0)
            def _():
                z_copy(p_ag, way, k + 1, j, block, block).start()

        @pl.when(jnp.logical_not(ag) & (i >= 0) & (i < h))
        def _():
            s = n - 1 - i if way == 0 else i
            term = partial(p_rs, s, j)
            block = rs.at[p_rs, way, s, rows_at(j), :]

            @pl.when(d > 0)
            def _():
                z_copy(p_rs, way, d + i, j, block, block).wait_recv()
                rs[p_rs, way, s, rows_at(j), :] = (
                    term + rs[p_rs, way, s, rows_at(j), :].astype(F32)
                ).astype(BF16)

            @pl.when(d == 0)
            def _():
                rs[p_rs, way, s, rows_at(j), :] = term.astype(BF16)

            z_copy(p_rs, way, d + i + 1, j, block, block).start()

        @pl.when(jnp.logical_not(ag) & (i == h) & (d > 0))
        def _():
            take_own(p_rs, way, j)

    def take_own(p, way, j):
        block = rs.at[p, way, r, rows_at(j), :]
        z_copy(p, way, n - 1, j, block, block).wait_recv()
        total[p, rows_at(j), :] += rs[p, way, r, rows_at(j), :].astype(F32)

    def term_step(s):
        d = jnp.where(s < r, r, n - 1 - r)
        distance = jnp.where(s < r, r - s, s - r)
        return jnp.where(s == r, n - 1, jnp.maximum(d + distance, n - 1))

    def one_step(step, _):
        def body(j, _):
            for way in range(2):
                arrivals(step, way, j)
            return 0

        lax.fori_loop(0, chunks, body, 0)
        for way in range(2):
            @pl.when((depth[way] == step) & has_next[way])
            def _(way=way):
                send_own(1, way)

        @pl.when(step == 1)
        def _():
            spread_pass(0)
            spread_end(0)
            spread_start(1)

        @pl.when(step == 2)
        def _():
            own_partial(0)

        @pl.when(step == n - 1)
        def _():
            spread_pass(1)
            lax.fori_loop(0, n_fs, make_grad_pre, 0)
            spread_end(1)

        @pl.when(step == n + 1)
        def _():
            own_partial(1)

        def terms(s, _):
            @pl.when(term_step(s) == step)
            def _():
                block_term(s)

            @pl.when(term_step(s) + 1 == step)
            def _():
                chip_sum(s)
            return 0

        lax.fori_loop(0, n, terms, 0)
        return 0

    lax.fori_loop(1, 2 * n, one_step, 0)
    gd_ref[...] = total[0].astype(gd_ref.dtype)

    def last(j, _):
        for way in range(2):
            @pl.when(depth[way] > 0)
            def _(way=way):
                take_own(1, way, j)
        gu_ref[rows_at(j), :] = total[1, rows_at(j), :].astype(gu_ref.dtype)
        return 0

    lax.fori_loop(0, chunks - 1, last, 0)
    own_rows = pl.ds(pl.multiple_of(f * tok, tok), tok)
    for s in range(n):
        acc = prec[s, own_rows, :].astype(F32)
        for d in range(1, n_fs):
            out_copy(s, d).wait()
            acc += frec[s, d - 1].astype(F32)
        gin_ref[:, s * shard:(s + 1) * shard] = acc.astype(BF16)
    for way in range(2):
        @pl.when(has_next[way])
        def _(way=way):
            def body(k, _):
                for p in range(2):
                    for j in range(chunks):
                        block = rs.at[0, 0, 0, rows_at(j), :]
                        z_copy(p, way, k, j, block, block).wait_send()
                return 0

            lax.fori_loop(0, n, body, 0)
    lax.fori_loop(chunks - 1, chunks, last, 0)


def on_device(n, n_fs, inputs, out_grad, pre_act, w_up, w_down_t):
    tok, d_model = inputs.shape
    group, cols = pre_act.shape
    shard = w_up.shape[0]
    chunks = max(1, shard // 128)
    factor = float(group * n) ** -0.5
    dma = pltpu.SemaphoreType.DMA
    vmem = pl.BlockSpec(memory_space=pltpu.VMEM)
    grad_in, grad_up, grad_down_t = pl.pallas_call(
        functools.partial(kernel, n, n_fs, chunks, factor),
        out_shape=(
            jax.ShapeDtypeStruct((tok, d_model), BF16),
            jax.ShapeDtypeStruct((shard, cols), BF16),
            jax.ShapeDtypeStruct((shard, cols), BF16),
        ),
        in_specs=[pl.BlockSpec(memory_space=pl.ANY)] * 5,
        out_specs=(vmem,) * 3,
        scratch_shapes=[
            pltpu.VMEM((2, group, d_model), BF16),
            pltpu.VMEM((2, n, shard, cols), BF16),
            pltpu.VMEM((2, group, cols), BF16),
            pltpu.VMEM((2, 2, n, shard, cols), BF16),
            pltpu.VMEM((n, 2, n_fs * tok, shard), BF16),
            pltpu.VMEM((n, n_fs * tok, shard), BF16),
            pltpu.VMEM((n, n_fs - 1, tok, shard), BF16),
            pltpu.VMEM((group, cols), BF16),
            pltpu.VMEM((2, shard, cols), F32),
            dma((2, 2, n, chunks)),
            dma((2, 2, n, chunks)),
            dma((2, n_fs)),
            dma((2, n_fs)),
            dma((2, n_fs)),
            dma((2, n_fs)),
            dma((n,)),
            dma((n,)),
            dma((n, n_fs)),
            dma((n, n_fs)),
            dma((5,)),
        ],
        compiler_params=pltpu.CompilerParams(
            collective_id=0, has_side_effects=True, vmem_limit_bytes=67043328
        ),
    )(inputs, out_grad, pre_act, w_up, w_down_t)
    return grad_in, grad_up.astype(F32), grad_down_t.astype(F32)


def solution(mesh):
    rows = P(("rep", "fs", "tp"), None)
    blocks = P("rep", ("fs", "tp"))
    return jax.shard_map(
        functools.partial(on_device, mesh.shape["rep"], mesh.shape["fs"]),
        mesh=mesh,
        in_specs=(rows, rows, blocks, blocks, blocks),
        out_specs=(rows, blocks, blocks),
        check_vma=False,
    )
```

time: 201 us -> 195 us (0.970)
  Pallas kernels: 195 us -> 189 us
    pallas_call x1, Pallas kernels: 195 us -> 189 us  [on_device(): pl.pallas_call(functools.partial(kernel, n, n_fs, chunks, factor), out_sh...]
where the time goes in v1:
time: 195 us
  Pallas kernels  189 us (97%)
  other arithmetic  4.44 us (2%)
    pallas_call x1, Pallas kernels, on_device(): pl.pallas_call(functools.partial(kernel, n, n_fs, chunks, factor), out_sh...  189 us
    convert_element_type x2, other arithmetic, on_device(): return (grad_in, grad_up.astype(F32), grad_down_t.astype(F32))  4.44 us

profile of v1, /device:TPU:0, one launch (start us, length us, event | category | flops | bytes accessed | tf_op | source)
XLA Modules:
  0.0 195.2 jit_solution(14868194604757358907)
XLA Ops:
  0.6 189.3 %shard_map.76 = (bf16[128,2048]{1,0:T(8,128)(2,1)}, bf16[512,1024]{1,0:T(8,128)(2,1)}, bf16[512,1024]{1,0:T(8,128)(2,1)}) custom-call(bf16[128,2048]{1,0:T(8,128)(2,1)} %x_ref.1, bf16[128,2048]{1,0:T(8,128)(2,1)} %og_ref.1, bf16[1024,1024]{1,0:T(8,128)(2,1)} %pre_ref.1, bf16[512,1024]{1,0:T(8,128)(2,1)} %wu_ref.1, bf16[512,1024]{1,0:T(8,128)(2,1)} %wd_ref.1), custom_call_target="tpu_custom_call" | custom-call | tf_op jit(solution)/shard_map/pallas_call | solution.py:328
  190.0 0.0 copy-start
  190.0 2.9 %convert_element_type.6 = f32[512,1024]{1,0:T(8,128)} convert(bf16[512,1024]{1,0:T(8,128)(2,1)} %get-tuple-element.7) | non-fusion elementwise | flops 524288 | bytes 3145728 | tf_op jit(solution)/shard_map/convert_element_type | solution.py:363
  192.9 0.0 copy-done
  192.9 0.0 copy-start.1
  192.9 1.6 convert_element_type.7
  194.4 0.0 copy-done.1
  194.4 0.8 copy.9
Async XLA Ops:
  190.0 2.9 %copy-start = (bf16[512,1024]{1,0:T(8,128)(2,1)S(1)}, bf16[512,1024]{1,0:T(8,128)(2,1)}, u32[]{:S(2)}) copy-start(bf16[512,1024]{1,0:T(8,128)(2,1)} %get-tuple-element.8) | copy-start | bytes 3145732
  192.9 1.6 copy-start.1

commit v2 on v1

--- a/solution.py
+++ b/solution.py
@@ -15,7 +15,7 @@
     n, n_fs, chunks, factor,
     x_ref, og_ref, pre_ref, wu_ref, wd_ref,
     gin_ref, gu_ref, gd_ref,
-    rows_all, w_all, act, rs, tbuf, prec, frec, pre, total,
+    rows_all, w_all, act, rs, tbuf, prec, frec, pre,
     zs, zr, xs, xr, cs, cr, ts, tr, fsend, frecv, ls,
 ):
     r, f, t = lax.axis_index("rep"), lax.axis_index("fs"), lax.axis_index("tp")
@@ -24,18 +24,19 @@
     crow = shard // chunks
     partner = {"tp": 1 - t}
     own_tokens = pl.ds(pl.multiple_of((f * 2 + t) * tok, tok), tok)
-    own_rows_of = (og_ref, x_ref)
-    own_w = (wd_ref, wu_ref)
+    totals = (gd_ref, gu_ref)
     loads = [
         pltpu.make_async_copy(src, dst, ls.at[i])
         for i, (src, dst) in enumerate((
+            (wd_ref, w_all.at[0, r]),
+            (og_ref, rows_all.at[0, own_tokens, :]),
+            (wu_ref, w_all.at[1, r]),
             (pre_ref, pre),
-            (og_ref, rows_all.at[0, own_tokens, :]),
             (x_ref, rows_all.at[1, own_tokens, :]),
-            (wd_ref, w_all.at[0, r]),
-            (wu_ref, w_all.at[1, r]),
         ))
     ]
+    for load in loads:
+        load.start()
     peers = [None] + [{"fs": lax.rem(f + d, n_fs)} for d in range(1, n_fs)]
     ahead = ({"rep": lax.rem(r + 1, n)}, {"rep": lax.rem(r + n - 1, n)})
     depth = (r, n - 1 - r)
@@ -50,6 +51,8 @@
     for d in range(1, n_fs):
         pl.semaphore_signal(barrier, inc=1, device_id=peers[d])
     pl.semaphore_signal(barrier, inc=1, device_id=partner)
+    for load in loads[:3]:
+        load.wait()
     pl.semaphore_wait(
         barrier, n_fs + jnp.where(r > 0, 1, 0) + jnp.where(r < n - 1, 1, 0)
     )
@@ -75,18 +78,16 @@
 
     def send_own(p, way):
         for j in range(chunks):
-            z_copy(
-                p, way, 0, j,
-                own_w[p].at[rows_at(j), :], w_all.at[p, r, rows_at(j), :],
-            ).start()
+            block = w_all.at[p, r, rows_at(j), :]
+            z_copy(p, way, 0, j, block, block).start()
 
     def spread_start(q):
-        own = own_rows_of[q]
+        own = rows_of(q, f, t)
         for d in range(1, n_fs):
             remote(
-                own, rows_of(q, f, t), xs.at[q, d], xr.at[q, d], peers[d]
+                own, own, xs.at[q, d], xr.at[q, d], peers[d]
             ).start()
-        remote(own, rows_of(q, f, t), cs.at[q, 0], cr.at[q, 0], partner).start()
+        remote(own, own, cs.at[q, 0], cr.at[q, 0], partner).start()
 
     def spread_pass(q):
         for d in range(1, n_fs):
@@ -108,9 +109,7 @@
         @pl.when(depth[way] == 0)
         def _(way=way):
             send_own(1, way)
-    for load in loads:
-        load.start()
-    for load in loads:
+    for load in loads[3:]:
         load.wait()
     tile = 2 * tok
 
@@ -131,7 +130,7 @@
 
     def own_partial(p):
         def body(j, _):
-            total[p, rows_at(j), :] = partial(p, r, j)
+            totals[p][rows_at(j), :] = partial(p, r, j)
             return 0
 
         lax.fori_loop(0, chunks, body, 0)
@@ -227,12 +226,12 @@
 
         @pl.when(jnp.logical_not(ag) & (i == h) & (d > 0))
         def _():
-            take_own(p_rs, way, j)
+            take_own(0, way, j)
 
     def take_own(p, way, j):
         block = rs.at[p, way, r, rows_at(j), :]
         z_copy(p, way, n - 1, j, block, block).wait_recv()
-        total[p, rows_at(j), :] += rs[p, way, r, rows_at(j), :].astype(F32)
+        totals[p][rows_at(j), :] += rs[p, way, r, rows_at(j), :].astype(F32)
 
     def term_step(s):
         d = jnp.where(s < r, r, n - 1 - r)
@@ -285,14 +284,12 @@
         return 0
 
     lax.fori_loop(1, 2 * n, one_step, 0)
-    gd_ref[...] = total[0].astype(gd_ref.dtype)
 
     def last(j, _):
         for way in range(2):
             @pl.when(depth[way] > 0)
             def _(way=way):
                 take_own(1, way, j)
-        gu_ref[rows_at(j), :] = total[1, rows_at(j), :].astype(gu_ref.dtype)
         return 0
 
     lax.fori_loop(0, chunks - 1, last, 0)
@@ -317,6 +314,16 @@
     lax.fori_loop(chunks - 1, chunks, last, 0)
 
 
+def write_out(*refs):
+    copies = [
+        pltpu.make_async_copy(refs[i], refs[3 + i], refs[6].at[i]) for i in range(3)
+    ]
+    for copy in copies:
+        copy.start()
+    for copy in copies:
+        copy.wait()
+
+
 def on_device(n, n_fs, inputs, out_grad, pre_act, w_up, w_down_t):
     tok, d_model = inputs.shape
     group, cols = pre_act.shape
@@ -325,12 +332,12 @@
     factor = float(group * n) ** -0.5
     dma = pltpu.SemaphoreType.DMA
     vmem = pl.BlockSpec(memory_space=pltpu.VMEM)
-    grad_in, grad_up, grad_down_t = pl.pallas_call(
+    results = pl.pallas_call(
         functools.partial(kernel, n, n_fs, chunks, factor),
         out_shape=(
-            jax.ShapeDtypeStruct((tok, d_model), BF16),
-            jax.ShapeDtypeStruct((shard, cols), BF16),
-            jax.ShapeDtypeStruct((shard, cols), BF16),
+            pltpu.VMEM((tok, d_model), BF16),
+            pltpu.VMEM((shard, cols), F32),
+            pltpu.VMEM((shard, cols), F32),
         ),
         in_specs=[pl.BlockSpec(memory_space=pl.ANY)] * 5,
         out_specs=(vmem,) * 3,
@@ -343,7 +350,6 @@
             pltpu.VMEM((n, n_fs * tok, shard), BF16),
             pltpu.VMEM((n, n_fs - 1, tok, shard), BF16),
             pltpu.VMEM((group, cols), BF16),
-            pltpu.VMEM((2, shard, cols), F32),
             dma((2, 2, n, chunks)),
             dma((2, 2, n, chunks)),
             dma((2, n_fs)),
@@ -357,10 +363,18 @@
             dma((5,)),
         ],
         compiler_params=pltpu.CompilerParams(
-            collective_id=0, has_side_effects=True, vmem_limit_bytes=67043328
+            collective_id=0, has_side_effects=True, vmem_limit_bytes=56 * 2**20
         ),
     )(inputs, out_grad, pre_act, w_up, w_down_t)
-    return grad_in, grad_up.astype(F32), grad_down_t.astype(F32)
+    results = [pltpu.with_memory_space_constraint(a, pltpu.VMEM) for a in results]
+    return pl.pallas_call(
+        write_out,
+        out_shape=[jax.ShapeDtypeStruct(a.shape, a.dtype) for a in results],
+        in_specs=[vmem] * 3,
+        out_specs=[pl.BlockSpec(memory_space=pl.ANY)] * 3,
+        scratch_shapes=[dma((3,))],
+        compiler_params=pltpu.CompilerParams(vmem_limit_bytes=2**20),
+    )(*results)
 
 
 def solution(mesh):

time: 195 us -> 191 us (0.979)
  other arithmetic: 4.44 us -> 0 us
    convert_element_type x2 -> x0, other arithmetic: 4.44 us -> none  [on_device(): return (grad_in, grad_up.astype(F32), grad_down_t.astype(F32))]
    pallas_call x0 -> x1, Pallas kernels: none -> 2.21 us  [on_device(): pl.pallas_call(write_out, out_shape=[jax.ShapeDtypeStruct(a.shape, a.dtyp...]
where the time goes in v2:
time: 191 us; the launch traced here: 190 us
  Pallas kernels  190 us (99%)
    pallas_call x1, Pallas kernels, on_device(): pl.pallas_call(functools.partial(kernel, n, n_fs, chunks, factor), out_sh...  188 us

profile of v2, /device:TPU:0, one launch (start us, length us, event | category | flops | bytes accessed | tf_op | source)
XLA Modules:
  0.0 190.4 jit_solution(11261310417862129119)
XLA Ops:
  0.6 187.6 %shard_map.76 = (bf16[128,2048]{1,0:T(8,128)(2,1)S(1)}, f32[512,1024]{1,0:T(8,128)S(1)}, f32[512,1024]{1,0:T(8,128)S(1)}) custom-call(bf16[128,2048]{1,0:T(8,128)(2,1)} %x_ref.1, bf16[128,2048]{1,0:T(8,128)(2,1)} %og_ref.1, bf16[1024,1024]{1,0:T(8,128)(2,1)} %pre_ref.1, bf16[512,1024]{1,0:T(8,128)(2,1)} %wu_ref.1, bf16[512,1024]{1,0:T(8,128)(2,1)} %wd_ref.1), custom_call_target="tpu_custom_call" | custom-call | tf_op jit(solution)/shard_map/pallas_call | solution.py:335
  188.2 2.2 %shard_map.77 = (bf16[128,2048]{1,0:T(8,128)(2,1)}, f32[512,1024]{1,0:T(8,128)}, f32[512,1024]{1,0:T(8,128)}) custom-call(bf16[128,2048]{1,0:T(8,128)(2,1)S(1)} %get-tuple-element.6.refs_0_, f32[512,1024]{1,0:T(8,128)S(1)} %get-tuple-element.7.refs_1_, f32[512,1024]{1,0:T(8,128)S(1)} %get-tuple-element.8.refs_2_), custom_call_target="tpu_custom_call" | custom-call | tf_op jit(solution)/shard_map/pallas_call | solution.py:370

commit v3 on v2

--- a/solution.py
+++ b/solution.py
@@ -35,8 +35,6 @@
             (x_ref, rows_all.at[1, own_tokens, :]),
         ))
     ]
-    for load in loads:
-        load.start()
     peers = [None] + [{"fs": lax.rem(f + d, n_fs)} for d in range(1, n_fs)]
     ahead = ({"rep": lax.rem(r + 1, n)}, {"rep": lax.rem(r + n - 1, n)})
     depth = (r, n - 1 - r)
@@ -51,8 +49,9 @@
     for d in range(1, n_fs):
         pl.semaphore_signal(barrier, inc=1, device_id=peers[d])
     pl.semaphore_signal(barrier, inc=1, device_id=partner)
-    for load in loads[:3]:
-        load.wait()
+    for load in loads:
+        load.start()
+    loads[0].wait()
     pl.semaphore_wait(
         barrier, n_fs + jnp.where(r > 0, 1, 0) + jnp.where(r < n - 1, 1, 0)
     )
@@ -70,7 +69,7 @@
 
     def z_copy(p, way, k, j, src, dst):
         return remote(
-            src, dst, zs.at[p, way, k, j], zr.at[p, way, k, j], ahead[way]
+            src, dst, zs.at[way], zr.at[p, way, k, j], ahead[way]
         )
 
     def rows_at(j):
@@ -81,30 +80,36 @@
             block = w_all.at[p, r, rows_at(j), :]
             z_copy(p, way, 0, j, block, block).start()
 
+    def first_rows(q, count):
+        return rows_all.at[q, pl.ds(0, count * tok), :]
+
+    def spread(q, block, d):
+        return remote(block, block, xs.at[q], xr.at[q], peers[d])
+
+    def swap(q, block):
+        return remote(block, block, cs.at[q], cr.at[q], partner)
+
     def spread_start(q):
         own = rows_of(q, f, t)
         for d in range(1, n_fs):
-            remote(
-                own, own, xs.at[q, d], xr.at[q, d], peers[d]
-            ).start()
-        remote(own, own, cs.at[q, 0], cr.at[q, 0], partner).start()
+            spread(q, own, d).start()
+        swap(q, own).start()
 
     def spread_pass(q):
+        spread(q, first_rows(q, n_fs - 1), 1).wait_recv()
         for d in range(1, n_fs):
-            src = rows_of(q, lax.rem(f + n_fs - d, n_fs), t)
-            remote(src, src, xs.at[q, d], xr.at[q, d], peers[d]).wait()
-            remote(src, src, cs.at[q, d], cr.at[q, d], partner).start()
+            swap(q, rows_of(q, lax.rem(f + d, n_fs), t)).start()
 
     def spread_end(q):
-        for d in range(n_fs):
-            there = rows_of(q, lax.rem(f + n_fs - d, n_fs), 1 - t)
-            remote(there, there, cs.at[q, d], cr.at[q, d], partner).wait()
+        swap(q, first_rows(q, n_fs)).wait_recv()
 
     for way in range(2):
         @pl.when(has_next[way])
         def _(way=way):
             send_own(0, way)
+    loads[1].wait()
     spread_start(0)
+    loads[2].wait()
     for way in range(2):
         @pl.when(depth[way] == 0)
         def _(way=way):
@@ -148,13 +153,13 @@
         return 0
 
     def cross(s):
-        return remote(tbuf.at[s, 1 - t], prec.at[s], ts.at[s], tr.at[s], partner)
+        return remote(tbuf.at[s, 1 - t], prec.at[s], ts, tr.at[s], partner)
 
     def out_copy(s, d):
         rows = pl.ds(pl.multiple_of(lax.rem(f + d, n_fs) * tok, tok), tok)
         return remote(
             prec.at[s, rows, :], frec.at[s, d - 1],
-            fsend.at[s, d], frecv.at[s, d], peers[d],
+            fsend, frecv, peers[d],
         )
 
     def block_term(s):
@@ -173,7 +178,7 @@
         cross(s).start()
 
     def chip_sum(s):
-        cross(s).wait()
+        cross(s).wait_recv()
 
         def body(i, _):
             here = pl.ds(pl.multiple_of(i * tok, tok), tok)
@@ -294,23 +299,20 @@
 
     lax.fori_loop(0, chunks - 1, last, 0)
     own_rows = pl.ds(pl.multiple_of(f * tok, tok), tok)
+    remote(frec, frec, fsend, frecv, peers[1]).wait()
     for s in range(n):
         acc = prec[s, own_rows, :].astype(F32)
         for d in range(1, n_fs):
-            out_copy(s, d).wait()
             acc += frec[s, d - 1].astype(F32)
         gin_ref[:, s * shard:(s + 1) * shard] = acc.astype(BF16)
+    remote(prec, prec, ts, tr.at[0], partner).wait_send()
+    for q in range(2):
+        spread(q, first_rows(q, n_fs - 1), 1).wait_send()
+        swap(q, first_rows(q, n_fs)).wait_send()
     for way in range(2):
         @pl.when(has_next[way])
         def _(way=way):
-            def body(k, _):
-                for p in range(2):
-                    for j in range(chunks):
-                        block = rs.at[0, 0, 0, rows_at(j), :]
-                        z_copy(p, way, k, j, block, block).wait_send()
-                return 0
-
-            lax.fori_loop(0, n, body, 0)
+            remote(w_all, w_all, zs.at[way], zr.at[0, way, 0, 0], ahead[way]).wait_send()
     lax.fori_loop(chunks - 1, chunks, last, 0)
 
 
@@ -328,7 +330,7 @@
     tok, d_model = inputs.shape
     group, cols = pre_act.shape
     shard = w_up.shape[0]
-    chunks = max(1, shard // 128)
+    chunks = max(1, shard // 256)
     factor = float(group * n) ** -0.5
     dma = pltpu.SemaphoreType.DMA
     vmem = pl.BlockSpec(memory_space=pltpu.VMEM)
@@ -350,16 +352,16 @@
             pltpu.VMEM((n, n_fs * tok, shard), BF16),
             pltpu.VMEM((n, n_fs - 1, tok, shard), BF16),
             pltpu.VMEM((group, cols), BF16),
+            dma((2,)),
             dma((2, 2, n, chunks)),
-            dma((2, 2, n, chunks)),
-            dma((2, n_fs)),
-            dma((2, n_fs)),
-            dma((2, n_fs)),
-            dma((2, n_fs)),
+            dma((2,)),
+            dma((2,)),
+            dma((2,)),
+            dma((2,)),
+            dma(()),
             dma((n,)),
-            dma((n,)),
-            dma((n, n_fs)),
-            dma((n, n_fs)),
+            dma(()),
+            dma(()),
             dma((5,)),
         ],
         compiler_params=pltpu.CompilerParams(

time: 191 us -> 189 us (0.990)
  Pallas kernels: 190 us -> 188 us
where the time goes in v3:
time: 189 us
  Pallas kernels  188 us (99%)
    pallas_call x1, Pallas kernels, on_device(): pl.pallas_call(functools.partial(kernel, n, n_fs, chunks, factor), out_sh...  186 us

profile of v3, /device:TPU:0, one launch (start us, length us, event | category | flops | bytes accessed | tf_op | source)
XLA Modules:
  0.0 189.1 jit_solution(110818383682493077)
XLA Ops:
  0.6 186.3 %shard_map.76 = (bf16[128,2048]{1,0:T(8,128)(2,1)S(1)}, f32[512,1024]{1,0:T(8,128)S(1)}, f32[512,1024]{1,0:T(8,128)S(1)}) custom-call(bf16[128,2048]{1,0:T(8,128)(2,1)} %x_ref.1, bf16[128,2048]{1,0:T(8,128)(2,1)} %og_ref.1, bf16[1024,1024]{1,0:T(8,128)(2,1)} %pre_ref.1, bf16[512,1024]{1,0:T(8,128)(2,1)} %wu_ref.1, bf16[512,1024]{1,0:T(8,128)(2,1)} %wd_ref.1), custom_call_target="tpu_custom_call" | custom-call | tf_op jit(solution)/shard_map/pallas_call | solution.py:337
  186.9 2.2 %shard_map.77 = (bf16[128,2048]{1,0:T(8,128)(2,1)}, f32[512,1024]{1,0:T(8,128)}, f32[512,1024]{1,0:T(8,128)}) custom-call(bf16[128,2048]{1,0:T(8,128)(2,1)S(1)} %get-tuple-element.6.refs_0_, f32[512,1024]{1,0:T(8,128)S(1)} %get-tuple-element.7.refs_1_, f32[512,1024]{1,0:T(8,128)S(1)} %get-tuple-element.8.refs_2_), custom_call_target="tpu_custom_call" | custom-call | tf_op jit(solution)/shard_map/pallas_call | solution.py:372

commit v4 on v3

--- a/solution.py
+++ b/solution.py
@@ -23,6 +23,7 @@
     shard, cols = wd_ref.shape
     crow = shard // chunks
     partner = {"tp": 1 - t}
+    half = tok // 2
     own_tokens = pl.ds(pl.multiple_of((f * 2 + t) * tok, tok), tok)
     totals = (gd_ref, gu_ref)
     loads = [
@@ -35,7 +36,8 @@
             (x_ref, rows_all.at[1, own_tokens, :]),
         ))
     ]
-    peers = [None] + [{"fs": lax.rem(f + d, n_fs)} for d in range(1, n_fs)]
+    peer = [None, f + 1 - 2 * lax.rem(f, 2), lax.rem(f + 2, n_fs), n_fs - 1 - f]
+    peers = [None] + [{"fs": peer[d]} for d in range(1, n_fs)]
     ahead = ({"rep": lax.rem(r + 1, n)}, {"rep": lax.rem(r + n - 1, n)})
     depth = (r, n - 1 - r)
     after = (n - 1 - r, r)
@@ -46,14 +48,14 @@
         @pl.when(has_next[way])
         def _(way=way):
             pl.semaphore_signal(barrier, inc=1, device_id=ahead[way])
-    for d in range(1, n_fs):
+    for d in (1, 2):
         pl.semaphore_signal(barrier, inc=1, device_id=peers[d])
     pl.semaphore_signal(barrier, inc=1, device_id=partner)
     for load in loads:
         load.start()
     loads[0].wait()
     pl.semaphore_wait(
-        barrier, n_fs + jnp.where(r > 0, 1, 0) + jnp.where(r < n - 1, 1, 0)
+        barrier, 3 + jnp.where(r > 0, 1, 0) + jnp.where(r < n - 1, 1, 0)
     )
 
     def remote(src, dst, send, recv, target):
@@ -83,38 +85,47 @@
     def first_rows(q, count):
         return rows_all.at[q, pl.ds(0, count * tok), :]
 
-    def spread(q, block, d):
-        return remote(block, block, xs.at[q], xr.at[q], peers[d])
+    def half_rows(q, ff, side):
+        at = (ff * 2 + t) * tok + side * half
+        return rows_all.at[q, pl.ds(pl.multiple_of(at, half), half), :]
+
+    def spread(q, block, d, stage):
+        return remote(block, block, xs.at[q], xr.at[q, stage], peers[d])
 
     def swap(q, block):
         return remote(block, block, cs.at[q], cr.at[q], partner)
 
     def spread_start(q):
         own = rows_of(q, f, t)
-        for d in range(1, n_fs):
-            spread(q, own, d).start()
+        for d in (1, 2):
+            spread(q, own, d, 0).start()
         swap(q, own).start()
 
+    def spread_relay(q):
+        spread(q, first_rows(q, 2), 1, 0).wait_recv()
+        spread(q, half_rows(q, peer[2], 0), 1, 1).start()
+        spread(q, half_rows(q, peer[1], 1), 2, 1).start()
+        for d in (1, 2):
+            swap(q, rows_of(q, peer[d], t)).start()
+
     def spread_pass(q):
-        spread(q, first_rows(q, n_fs - 1), 1).wait_recv()
-        for d in range(1, n_fs):
-            swap(q, rows_of(q, lax.rem(f + d, n_fs), t)).start()
+        spread(q, first_rows(q, 1), 1, 1).wait_recv()
+        swap(q, rows_of(q, peer[3], t)).start()
 
     def spread_end(q):
         swap(q, first_rows(q, n_fs)).wait_recv()
 
-    for way in range(2):
-        @pl.when(has_next[way])
-        def _(way=way):
-            send_own(0, way)
+    def first_sends():
+        for way in range(2):
+            @pl.when(has_next[way])
+            def _(way=way):
+                send_own(0, way)
+
+    first_sends()
+
     loads[1].wait()
     spread_start(0)
-    loads[2].wait()
-    for way in range(2):
-        @pl.when(depth[way] == 0)
-        def _(way=way):
-            send_own(1, way)
-    for load in loads[3:]:
+    for load in loads[2:]:
         load.wait()
     tile = 2 * tok
 
@@ -125,6 +136,12 @@
         return 0
 
     lax.fori_loop(0, n_fs, square, 0)
+
+
+    for way in range(2):
+        @pl.when(depth[way] == 0)
+        def _(way=way):
+            send_own(1, way)
 
     def partial(p, s, j):
         at = pl.ds(pl.multiple_of(s * shard + j * crow, crow), crow)
@@ -156,7 +173,7 @@
         return remote(tbuf.at[s, 1 - t], prec.at[s], ts, tr.at[s], partner)
 
     def out_copy(s, d):
-        rows = pl.ds(pl.multiple_of(lax.rem(f + d, n_fs) * tok, tok), tok)
+        rows = pl.ds(pl.multiple_of(peer[d] * tok, tok), tok)
         return remote(
             prec.at[s, rows, :], frec.at[s, d - 1],
             fsend, frecv, peers[d],
@@ -247,6 +264,10 @@
         def body(j, _):
             for way in range(2):
                 arrivals(step, way, j)
+
+            @pl.when((step <= 2) & (j == 0))
+            def _():
+                spread_relay(step - 1)
             return 0
 
         lax.fori_loop(0, chunks, body, 0)
@@ -257,9 +278,9 @@
 
         @pl.when(step == 1)
         def _():
+            spread_start(1)
             spread_pass(0)
             spread_end(0)
-            spread_start(1)
 
         @pl.when(step == 2)
         def _():
@@ -307,7 +328,7 @@
         gin_ref[:, s * shard:(s + 1) * shard] = acc.astype(BF16)
     remote(prec, prec, ts, tr.at[0], partner).wait_send()
     for q in range(2):
-        spread(q, first_rows(q, n_fs - 1), 1).wait_send()
+        spread(q, first_rows(q, n_fs - 1), 1, 0).wait_send()
         swap(q, first_rows(q, n_fs)).wait_send()
     for way in range(2):
         @pl.when(has_next[way])
@@ -355,7 +376,7 @@
             dma((2,)),
             dma((2, 2, n, chunks)),
             dma((2,)),
-            dma((2,)),
+            dma((2, 2)),
             dma((2,)),
             dma((2,)),
             dma(()),

time: 189 us -> 188 us (level)
  no operation moved by 1% of the time
where the time goes in v4:
time: 188 us
  Pallas kernels  188 us (100%)
    pallas_call x1, Pallas kernels, on_device(): pl.pallas_call(functools.partial(kernel, n, n_fs, chunks, factor), out_sh...  185 us

profile of v4, /device:TPU:0, one launch (start us, length us, event | category | flops | bytes accessed | tf_op | source)
XLA Modules:
  0.0 188.3 jit_solution(15851878370946141911)
XLA Ops:
  0.6 185.4 %shard_map.76 = (bf16[128,2048]{1,0:T(8,128)(2,1)S(1)}, f32[512,1024]{1,0:T(8,128)S(1)}, f32[512,1024]{1,0:T(8,128)S(1)}) custom-call(bf16[128,2048]{1,0:T(8,128)(2,1)} %x_ref.1, bf16[128,2048]{1,0:T(8,128)(2,1)} %og_ref.1, bf16[1024,1024]{1,0:T(8,128)(2,1)} %pre_ref.1, bf16[512,1024]{1,0:T(8,128)(2,1)} %wu_ref.1, bf16[512,1024]{1,0:T(8,128)(2,1)} %wd_ref.1), custom_call_target="tpu_custom_call" | custom-call | tf_op jit(solution)/shard_map/pallas_call | solution.py:358
  186.1 2.2 %shard_map.77 = (bf16[128,2048]{1,0:T(8,128)(2,1)}, f32[512,1024]{1,0:T(8,128)}, f32[512,1024]{1,0:T(8,128)}) custom-call(bf16[128,2048]{1,0:T(8,128)(2,1)S(1)} %get-tuple-element.6.refs_0_, f32[512,1024]{1,0:T(8,128)S(1)} %get-tuple-element.7.refs_1_, f32[512,1024]{1,0:T(8,128)S(1)} %get-tuple-element.8.refs_2_), custom_call_target="tpu_custom_call" | custom-call | tf_op jit(solution)/shard_map/pallas_call | solution.py:393

commit v5 on v4

--- a/solution.py
+++ b/solution.py
@@ -16,7 +16,7 @@
     x_ref, og_ref, pre_ref, wu_ref, wd_ref,
     gin_ref, gu_ref, gd_ref,
     rows_all, w_all, act, rs, tbuf, prec, frec, pre,
-    zs, zr, xs, xr, cs, cr, ts, tr, fsend, frecv, ls,
+    zs, zr, xs, xr, cs, cr, ts, tr, fsend, frecv, ls, ready,
 ):
     r, f, t = lax.axis_index("rep"), lax.axis_index("fs"), lax.axis_index("tp")
     tok, d_model = og_ref.shape
@@ -48,15 +48,35 @@
         @pl.when(has_next[way])
         def _(way=way):
             pl.semaphore_signal(barrier, inc=1, device_id=ahead[way])
-    for d in (1, 2):
-        pl.semaphore_signal(barrier, inc=1, device_id=peers[d])
-    pl.semaphore_signal(barrier, inc=1, device_id=partner)
+    inner = (f > 0) & (f < n_fs - 1)
+
+    @pl.when(jnp.logical_not(inner))
+    def _():
+        for d in (1, 2):
+            pl.semaphore_signal(barrier, inc=1, device_id=peers[d])
+
+    @pl.when(t == 0)
+    def _():
+        pl.semaphore_signal(barrier, inc=1, device_id=partner)
+
     for load in loads:
         load.start()
+    pl.semaphore_wait(
+        barrier,
+        jnp.where(r > 0, 1, 0) + jnp.where(r < n - 1, 1, 0)
+        + jnp.where(inner, 2, 0) + t,
+    )
+
+    @pl.when(inner)
+    def _():
+        for d in (1, 2):
+            pl.semaphore_signal(ready, inc=1, device_id=peers[d])
+
+    @pl.when(t == 1)
+    def _():
+        pl.semaphore_signal(ready, inc=1, device_id=partner)
+
     loads[0].wait()
-    pl.semaphore_wait(
-        barrier, 3 + jnp.where(r > 0, 1, 0) + jnp.where(r < n - 1, 1, 0)
-    )
 
     def remote(src, dst, send, recv, target):
         return pltpu.make_async_remote_copy(
@@ -77,8 +97,8 @@
     def rows_at(j):
         return pl.ds(pl.multiple_of(j * crow, crow), crow)
 
-    def send_own(p, way):
-        for j in range(chunks):
+    def send_own(p, way, pieces=range(chunks)):
+        for j in pieces:
             block = w_all.at[p, r, rows_at(j), :]
             z_copy(p, way, 0, j, block, block).start()
 
@@ -115,17 +135,35 @@
     def spread_end(q):
         swap(q, first_rows(q, n_fs)).wait_recv()
 
-    def first_sends():
+    def rest_of_first_sends():
         for way in range(2):
             @pl.when(has_next[way])
             def _(way=way):
-                send_own(0, way)
-
-    first_sends()
+                send_own(0, way, range(1, chunks))
+
+            @pl.when(depth[way] == 0)
+            def _(way=way):
+                send_own(1, way)
+
+    for way in range(2):
+        @pl.when(has_next[way])
+        def _(way=way):
+            send_own(0, way, range(1))
 
     loads[1].wait()
+
+    @pl.when(jnp.logical_not(inner) | (t == 0))
+    def _():
+        pl.semaphore_wait(ready, jnp.where(inner, 0, 2) + 1 - t)
+
     spread_start(0)
-    for load in loads[2:]:
+    loads[2].wait()
+
+    @pl.when(t == 0)
+    def _():
+        rest_of_first_sends()
+
+    for load in loads[3:]:
         load.wait()
     tile = 2 * tok
 
@@ -137,11 +175,6 @@
 
     lax.fori_loop(0, n_fs, square, 0)
 
-
-    for way in range(2):
-        @pl.when(depth[way] == 0)
-        def _(way=way):
-            send_own(1, way)
 
     def partial(p, s, j):
         at = pl.ds(pl.multiple_of(s * shard + j * crow, crow), crow)
@@ -268,6 +301,10 @@
             @pl.when((step <= 2) & (j == 0))
             def _():
                 spread_relay(step - 1)
+
+            @pl.when((step == 1) & (j == 0) & (t == 1))
+            def _():
+                rest_of_first_sends()
             return 0
 
         lax.fori_loop(0, chunks, body, 0)
@@ -384,6 +421,7 @@
             dma(()),
             dma(()),
             dma((5,)),
+            pltpu.SemaphoreType.REGULAR,
         ],
         compiler_params=pltpu.CompilerParams(
             collective_id=0, has_side_effects=True, vmem_limit_bytes=56 * 2**20

time: 188 us -> 188 us (level); the launches traced: 188 us -> 185 us
  Pallas kernels: 188 us -> 184 us
    pallas_call x1, Pallas kernels: 185 us -> 182 us  [on_device(): pl.pallas_call(functools.partial(kernel, n, n_fs, chunks, factor), out_sh...]
where the time goes in v5:
time: 188 us; the launch traced here: 185 us
  Pallas kernels  184 us (98%)
    pallas_call x1, Pallas kernels, on_device(): pl.pallas_call(functools.partial(kernel, n, n_fs, chunks, factor), out_sh...  182 us

profile of v5, /device:TPU:0, one launch (start us, length us, event | category | flops | bytes accessed | tf_op | source)
XLA Modules:
  0.0 184.8 jit_solution(2448517667479171862)
XLA Ops:
  0.6 181.9 %shard_map.76 = (bf16[128,2048]{1,0:T(8,128)(2,1)S(1)}, f32[512,1024]{1,0:T(8,128)S(1)}, f32[512,1024]{1,0:T(8,128)S(1)}) custom-call(bf16[128,2048]{1,0:T(8,128)(2,1)} %x_ref.1, bf16[128,2048]{1,0:T(8,128)(2,1)} %og_ref.1, bf16[1024,1024]{1,0:T(8,128)(2,1)} %pre_ref.1, bf16[512,1024]{1,0:T(8,128)(2,1)} %wu_ref.1, bf16[512,1024]{1,0:T(8,128)(2,1)} %wd_ref.1), custom_call_target="tpu_custom_call" | custom-call | tf_op jit(solution)/shard_map/pallas_call | solution.py:395
  182.5 2.2 %shard_map.77 = (bf16[128,2048]{1,0:T(8,128)(2,1)}, f32[512,1024]{1,0:T(8,128)}, f32[512,1024]{1,0:T(8,128)}) custom-call(bf16[128,2048]{1,0:T(8,128)(2,1)S(1)} %get-tuple-element.6.refs_0_, f32[512,1024]{1,0:T(8,128)S(1)} %get-tuple-element.7.refs_1_, f32[512,1024]{1,0:T(8,128)S(1)} %get-tuple-element.8.refs_2_), custom_call_target="tpu_custom_call" | custom-call | tf_op jit(solution)/shard_map/pallas_call | solution.py:431

commit v6 on v3

v6 whole, which is shorter than its diff:
```python
import functools

import jax
import jax.numpy as jnp
from jax import lax
from jax.experimental import pallas as pl
from jax.experimental.pallas import tpu as pltpu
from jax.sharding import PartitionSpec as P

BF16 = jnp.bfloat16
F32 = jnp.float32


def kernel(
    n, n_fs, chunks, factor,
    x_ref, og_ref, pre_ref, wu_ref, wd_ref,
    gin_ref, gu_ref, gd_ref,
    rows_all, w_all, act, rs, tbuf, prec, frec, pre,
    zs, z_last, fsend, frecv,
):
    r, f, t = lax.axis_index("rep"), lax.axis_index("fs"), lax.axis_index("tp")
    tok, d_model = og_ref.shape
    shard, cols = wd_ref.shape
    crow = shard // chunks
    partner = {"tp": 1 - t}
    half = tok // 2
    own_tokens = pl.ds(pl.multiple_of((f * 2 + t) * tok, tok), tok)
    totals = (gd_ref, gu_ref)
    peer = [None, f + 1 - 2 * lax.rem(f, 2), lax.rem(f + 2, n_fs), n_fs - 1 - f]
    peers = [None] + [{"fs": peer[d]} for d in range(1, n_fs)]
    ahead = ({"rep": lax.rem(r + 1, n)}, {"rep": lax.rem(r + n - 1, n)})
    depth = (r, n - 1 - r)
    after = (n - 1 - r, r)
    has_next = (r < n - 1, r > 0)

    def remote(src, dst, send, recv, target):
        return pltpu.make_async_remote_copy(
            src_ref=src, dst_ref=dst, send_sem=send, recv_sem=recv,
            device_id=target, device_id_type=pl.DeviceIdType.MESH,
        )

    def rows_at(j):
        return pl.ds(pl.multiple_of(j * crow, crow), crow)

    def z_final(way, s, j):
        block = rs.at[1, way, s, rows_at(j), :]
        return remote(block, block, zs.at[way], z_last.at[way, j], ahead[way])

    def all_but_last_step(zr, xs, xr, cs, cr, ts, tr, ls, ready):
        loads = [
            pltpu.make_async_copy(src, dst, ls.at[i])
            for i, (src, dst) in enumerate((
                (wd_ref, w_all.at[0, r]),
                (og_ref, rows_all.at[0, own_tokens, :]),
                (wu_ref, w_all.at[1, r]),
                (pre_ref, pre),
                (x_ref, rows_all.at[1, own_tokens, :]),
            ))
        ]
        barrier = pltpu.get_barrier_semaphore()
        for way in range(2):
            @pl.when(has_next[way])
            def _(way=way):
                pl.semaphore_signal(barrier, inc=1, device_id=ahead[way])
        inner = (f > 0) & (f < n_fs - 1)

        @pl.when(jnp.logical_not(inner))
        def _():
            for d in (1, 2):
                pl.semaphore_signal(barrier, inc=1, device_id=peers[d])

        @pl.when(t == 0)
        def _():
            pl.semaphore_signal(barrier, inc=1, device_id=partner)

        for load in loads:
            load.start()
        pl.semaphore_wait(
            barrier,
            jnp.where(r > 0, 1, 0) + jnp.where(r < n - 1, 1, 0)
            + jnp.where(inner, 2, 0) + t,
        )

        @pl.when(inner)
        def _():
            for d in (1, 2):
                pl.semaphore_signal(ready, inc=1, device_id=peers[d])

        @pl.when(t == 1)
        def _():
            pl.semaphore_signal(ready, inc=1, device_id=partner)

        loads[0].wait()

        def rows_of(q, ff, tt):
            return rows_all.at[
                q, pl.ds(pl.multiple_of((ff * 2 + tt) * tok, tok), tok), :
            ]

        def z_copy(p, way, k, j, src, dst):
            return remote(src, dst, zs.at[way], zr.at[p, way, k, j], ahead[way])

        def send_own(p, way, pieces=range(chunks)):
            for j in pieces:
                block = w_all.at[p, r, rows_at(j), :]
                z_copy(p, way, 0, j, block, block).start()

        def first_rows(q, count):
            return rows_all.at[q, pl.ds(0, count * tok), :]

        def half_rows(q, ff, side):
            at = (ff * 2 + t) * tok + side * half
            return rows_all.at[q, pl.ds(pl.multiple_of(at, half), half), :]

        def spread(q, block, d, stage):
            return remote(block, block, xs.at[q], xr.at[q, stage], peers[d])

        def swap(q, block):
            return remote(block, block, cs.at[q], cr.at[q], partner)

        def spread_start(q):
            own = rows_of(q, f, t)
            for d in (1, 2):
                spread(q, own, d, 0).start()
            swap(q, own).start()

        def spread_relay(q):
            spread(q, first_rows(q, 2), 1, 0).wait_recv()
            spread(q, half_rows(q, peer[2], 0), 1, 1).start()
            spread(q, half_rows(q, peer[1], 1), 2, 1).start()
            for d in (1, 2):
                swap(q, rows_of(q, peer[d], t)).start()

        def spread_pass(q):
            spread(q, first_rows(q, 1), 1, 1).wait_recv()
            swap(q, rows_of(q, peer[3], t)).start()

        def spread_end(q):
            swap(q, first_rows(q, n_fs)).wait_recv()

        def rest_of_first_sends():
            for way in range(2):
                @pl.when(has_next[way])
                def _(way=way):
                    send_own(0, way, range(1, chunks))

                @pl.when(depth[way] == 0)
                def _(way=way):
                    send_own(1, way)

        for way in range(2):
            @pl.when(has_next[way])
            def _(way=way):
                send_own(0, way, range(1))

        loads[1].wait()

        @pl.when(jnp.logical_not(inner) | (t == 0))
        def _():
            pl.semaphore_wait(ready, jnp.where(inner, 0, 2) + 1 - t)

        spread_start(0)
        loads[2].wait()

        @pl.when(t == 0)
        def _():
            rest_of_first_sends()

        for load in loads[3:]:
            load.wait()
        tile = 2 * tok

        def square(i, _):
            at = pl.ds(pl.multiple_of(i * tile, tile), tile)
            linear = jnp.maximum(pre[at, :].astype(F32), 0.0)
            act[0, at, :] = (linear * linear).astype(BF16)
            return 0

        lax.fori_loop(0, n_fs, square, 0)


        def partial(p, s, j):
            at = pl.ds(pl.multiple_of(s * shard + j * crow, crow), crow)
            return lax.dot_general(
                rows_all[p, :, at], act[p], (((0,), (0,)), ((), ())),
                preferred_element_type=F32,
            ) * factor

        def own_partial(p):
            def body(j, _):
                totals[p][rows_at(j), :] = partial(p, r, j)
                return 0

            lax.fori_loop(0, chunks, body, 0)

        def make_grad_pre(i, _):
            at = pl.ds(pl.multiple_of(i * tile, tile), tile)
            acc = jnp.zeros((tile, cols), F32)
            for s in range(n):
                acc += jnp.dot(
                    rows_all[0, at, s * shard:(s + 1) * shard], w_all[0, s],
                    preferred_element_type=F32,
                )
            linear = jnp.maximum(pre[at, :].astype(F32), 0.0)
            act[1, at, :] = (acc * 2.0 * linear).astype(BF16)
            return 0

        def cross(s):
            return remote(tbuf.at[s, 1 - t], prec.at[s], ts, tr.at[s], partner)

        def out_copy(s, d):
            rows = pl.ds(pl.multiple_of(peer[d] * tok, tok), tok)
            return remote(
                prec.at[s, rows, :], frec.at[s, d - 1],
                fsend, frecv, peers[d],
            )

        def block_term(s):
            def body(i, _):
                at = pl.ds(pl.multiple_of(i * tile, tile), tile)
                here = pl.ds(pl.multiple_of(i * tok, tok), tok)
                term = lax.dot_general(
                    act[1, at, :], w_all[1, s], (((1,), (1,)), ((), ())),
                    preferred_element_type=F32,
                ).astype(BF16)
                tbuf[s, 0, here, :] = term[:tok]
                tbuf[s, 1, here, :] = term[tok:]
                return 0

            lax.fori_loop(0, n_fs, body, 0)
            cross(s).start()

        def chip_sum(s):
            cross(s).wait_recv()

            def body(i, _):
                here = pl.ds(pl.multiple_of(i * tok, tok), tok)
                prec[s, here, :] = (
                    prec[s, here, :].astype(F32) + tbuf[s, t, here, :].astype(F32)
                ).astype(BF16)
                return 0

            lax.fori_loop(0, n_fs, body, 0)
            for d in range(1, n_fs):
                out_copy(s, d).start()

        def arrivals(step, way, j):
            d, h = depth[way], after[way]
            sign = 1 - 2 * way
            ag = step <= 2 * d
            p_ag = jnp.where(step > d, 1, 0)
            k = step - 1 - p_ag * d
            q = step - 2 * d - 1
            p_rs = jnp.where(q > h, 1, 0)
            i = q - p_rs * (h + 1) - jnp.where((d == 0) & (p_rs == 0), 1, 0)

            @pl.when(ag)
            def _():
                block = w_all.at[p_ag, r - sign * (1 + k), rows_at(j), :]
                z_copy(p_ag, way, k, j, block, block).wait_recv()

                @pl.when(h > 0)
                def _():
                    z_copy(p_ag, way, k + 1, j, block, block).start()

            @pl.when(jnp.logical_not(ag) & (i >= 0) & (i < h))
            def _():
                s = n - 1 - i if way == 0 else i
                term = partial(p_rs, s, j)
                block = rs.at[p_rs, way, s, rows_at(j), :]

                @pl.when(d > 0)
                def _():
                    z_copy(p_rs, way, d + i, j, block, block).wait_recv()
                    rs[p_rs, way, s, rows_at(j), :] = (
                        term + rs[p_rs, way, s, rows_at(j), :].astype(F32)
                    ).astype(BF16)

                @pl.when(d == 0)
                def _():
                    rs[p_rs, way, s, rows_at(j), :] = term.astype(BF16)

                final = (p_rs == 1) & (i == h - 1)

                @pl.when(final)
                def _():
                    z_final(way, s, j).start()

                @pl.when(jnp.logical_not(final))
                def _():
                    z_copy(p_rs, way, d + i + 1, j, block, block).start()

            @pl.when(jnp.logical_not(ag) & (i == h) & (d > 0))
            def _():
                block = rs.at[0, way, r, rows_at(j), :]
                z_copy(0, way, n - 1, j, block, block).wait_recv()
                gd_ref[rows_at(j), :] += rs[0, way, r, rows_at(j), :].astype(F32)

        def term_step(s):
            d = jnp.where(s < r, r, n - 1 - r)
            distance = jnp.where(s < r, r - s, s - r)
            return jnp.where(s == r, n - 1, jnp.maximum(d + distance, n - 1))

        def one_step(step, _):
            def body(j, _):
                for way in range(2):
                    arrivals(step, way, j)

                @pl.when((step <= 2) & (j == 0))
                def _():
                    spread_relay(step - 1)

                @pl.when((step == 1) & (j == 0) & (t == 1))
                def _():
                    rest_of_first_sends()
                return 0

            lax.fori_loop(0, chunks, body, 0)
            for way in range(2):
                @pl.when((depth[way] == step) & has_next[way])
                def _(way=way):
                    send_own(1, way)

            @pl.when(step == 1)
            def _():
                spread_start(1)
                spread_pass(0)
                spread_end(0)

            @pl.when(step == 2)
            def _():
                own_partial(0)

            @pl.when(step == n - 1)
            def _():
                spread_pass(1)
                lax.fori_loop(0, n_fs, make_grad_pre, 0)
                spread_end(1)

            @pl.when(step == n + 1)
            def _():
                own_partial(1)

            def terms(s, _):
                @pl.when(term_step(s) == step)
                def _():
                    block_term(s)

                @pl.when(term_step(s) + 1 == step)
                def _():
                    chip_sum(s)
                return 0

            lax.fori_loop(0, n, terms, 0)
            return 0

        lax.fori_loop(1, 2 * n, one_step, 0)
        remote(prec, prec, ts, tr.at[0], partner).wait_send()
        for q in range(2):
            spread(q, first_rows(q, n_fs - 1), 1, 0).wait_send()
            swap(q, first_rows(q, n_fs)).wait_send()

    dma = pltpu.SemaphoreType.DMA
    pl.run_scoped(
        all_but_last_step,
        dma((2, 2, n, chunks)), dma((2,)), dma((2, 2)), dma((2,)), dma((2,)),
        dma(()), dma((n,)), dma((5,)), pltpu.SemaphoreType.REGULAR,
    )

    def last(j, _):
        for way in range(2):
            @pl.when(depth[way] > 0)
            def _(way=way):
                z_final(way, r, j).wait_recv()
                gu_ref[rows_at(j), :] += rs[1, way, r, rows_at(j), :].astype(F32)
        return 0

    lax.fori_loop(0, chunks - 1, last, 0)
    own_rows = pl.ds(pl.multiple_of(f * tok, tok), tok)
    remote(frec, frec, fsend, frecv, peers[1]).wait()
    for s in range(n):
        acc = prec[s, own_rows, :].astype(F32)
        for d in range(1, n_fs):
            acc += frec[s, d - 1].astype(F32)
        gin_ref[:, s * shard:(s + 1) * shard] = acc.astype(BF16)
    for way in range(2):
        @pl.when(has_next[way])
        def _(way=way):
            remote(w_all, w_all, zs.at[way], z_last.at[way, 0], ahead[way]).wait_send()
    lax.fori_loop(chunks - 1, chunks, last, 0)


def write_out(*refs):
    copies = [
        pltpu.make_async_copy(refs[i], refs[3 + i], refs[6].at[i]) for i in range(3)
    ]
    for copy in copies:
        copy.start()
    for copy in copies:
        copy.wait()


def on_device(n, n_fs, inputs, out_grad, pre_act, w_up, w_down_t):
    tok, d_model = inputs.shape
    group, cols = pre_act.shape
    shard = w_up.shape[0]
    chunks = max(1, shard // 256)
    factor = float(group * n) ** -0.5
    dma = pltpu.SemaphoreType.DMA
    vmem = pl.BlockSpec(memory_space=pltpu.VMEM)
    results = pl.pallas_call(
        functools.partial(kernel, n, n_fs, chunks, factor),
        out_shape=(
            pltpu.VMEM((tok, d_model), BF16),
            pltpu.VMEM((shard, cols), F32),
            pltpu.VMEM((shard, cols), F32),
        ),
        in_specs=[pl.BlockSpec(memory_space=pl.ANY)] * 5,
        out_specs=(vmem,) * 3,
        scratch_shapes=[
            pltpu.VMEM((2, group, d_model), BF16),
            pltpu.VMEM((2, n, shard, cols), BF16),
            pltpu.VMEM((2, group, cols), BF16),
            pltpu.VMEM((2, 2, n, shard, cols), BF16),
            pltpu.VMEM((n, 2, n_fs * tok, shard), BF16),
            pltpu.VMEM((n, n_fs * tok, shard), BF16),
            pltpu.VMEM((n, n_fs - 1, tok, shard), BF16),
            pltpu.VMEM((group, cols), BF16),
            dma((2,)),
            dma((2, chunks)),
            dma(()),
            dma(()),
        ],
        compiler_params=pltpu.CompilerParams(
            collective_id=0, has_side_effects=True, vmem_limit_bytes=56 * 2**20
        ),
    )(inputs, out_grad, pre_act, w_up, w_down_t)
    results = [pltpu.with_memory_space_constraint(a, pltpu.VMEM) for a in results]
    return pl.pallas_call(
        write_out,
        out_shape=[jax.ShapeDtypeStruct(a.shape, a.dtype) for a in results],
        in_specs=[vmem] * 3,
        out_specs=[pl.BlockSpec(memory_space=pl.ANY)] * 3,
        scratch_shapes=[dma((3,))],
        compiler_params=pltpu.CompilerParams(vmem_limit_bytes=2**20),
    )(*results)


def solution(mesh):
    rows = P(("rep", "fs", "tp"), None)
    blocks = P("rep", ("fs", "tp"))
    return jax.shard_map(
        functools.partial(on_device, mesh.shape["rep"], mesh.shape["fs"]),
        mesh=mesh,
        in_specs=(rows, rows, blocks, blocks, blocks),
        out_specs=(rows, blocks, blocks),
        check_vma=False,
    )
```

time: 189 us -> 187 us (0.989); the launches traced: 189 us -> 184 us
  Pallas kernels: 188 us -> 184 us
    pallas_call x1, Pallas kernels: 186 us -> 181 us  [on_device(): pl.pallas_call(functools.partial(kernel, n, n_fs, chunks, factor), out_sh...]
where the time goes in v6:
time: 187 us; the launch traced here: 184 us
  Pallas kernels  184 us (98%)
    pallas_call x1, Pallas kernels, on_device(): pl.pallas_call(functools.partial(kernel, n, n_fs, chunks, factor), out_sh...  181 us

profile of v6, /device:TPU:0, one launch (start us, length us, event | category | flops | bytes accessed | tf_op | source)
XLA Modules:
  0.0 184.3 jit_solution(8532605255723193989)
XLA Ops:
  0.6 181.5 %shard_map.76 = (bf16[128,2048]{1,0:T(8,128)(2,1)S(1)}, f32[512,1024]{1,0:T(8,128)S(1)}, f32[512,1024]{1,0:T(8,128)S(1)}) custom-call(bf16[128,2048]{1,0:T(8,128)(2,1)} %x_ref.1, bf16[128,2048]{1,0:T(8,128)(2,1)} %og_ref.1, bf16[1024,1024]{1,0:T(8,128)(2,1)} %pre_ref.1, bf16[512,1024]{1,0:T(8,128)(2,1)} %wu_ref.1, bf16[512,1024]{1,0:T(8,128)(2,1)} %wd_ref.1), custom_call_target="tpu_custom_call" | custom-call | tf_op jit(solution)/shard_map/pallas_call | solution.py:411
  182.1 2.2 %shard_map.77 = (bf16[128,2048]{1,0:T(8,128)(2,1)}, f32[512,1024]{1,0:T(8,128)}, f32[512,1024]{1,0:T(8,128)}) custom-call(bf16[128,2048]{1,0:T(8,128)(2,1)S(1)} %get-tuple-element.6.refs_0_, f32[512,1024]{1,0:T(8,128)S(1)} %get-tuple-element.7.refs_1_, f32[512,1024]{1,0:T(8,128)S(1)} %get-tuple-element.8.refs_2_), custom_call_target="tpu_custom_call" | custom-call | tf_op jit(solution)/shard_map/pallas_call | solution.py:439

commit v7 on v6

--- a/solution.py
+++ b/solution.py
@@ -46,22 +46,24 @@
         block = rs.at[1, way, s, rows_at(j), :]
         return remote(block, block, zs.at[way], z_last.at[way, j], ahead[way])
 
-    def all_but_last_step(zr, xs, xr, cs, cr, ts, tr, ls, ready):
+    def all_but_last_step(zr, xs, xr, cs, cr, ts, tr, ls, ready, answer):
+        lead = crow + crow // 8 if chunks > 1 else crow // 2
         loads = [
             pltpu.make_async_copy(src, dst, ls.at[i])
             for i, (src, dst) in enumerate((
-                (wd_ref, w_all.at[0, r]),
+                (wd_ref.at[:lead], w_all.at[0, r, :lead]),
                 (og_ref, rows_all.at[0, own_tokens, :]),
                 (wu_ref, w_all.at[1, r]),
                 (pre_ref, pre),
                 (x_ref, rows_all.at[1, own_tokens, :]),
+                (wd_ref.at[lead:], w_all.at[0, r, lead:]),
             ))
         ]
         barrier = pltpu.get_barrier_semaphore()
-        for way in range(2):
-            @pl.when(has_next[way])
-            def _(way=way):
-                pl.semaphore_signal(barrier, inc=1, device_id=ahead[way])
+        @pl.when(has_next[0])
+        def _():
+            pl.semaphore_signal(barrier, inc=1, device_id=ahead[0])
+
         inner = (f > 0) & (f < n_fs - 1)
 
         @pl.when(jnp.logical_not(inner))
@@ -75,11 +77,15 @@
 
         for load in loads:
             load.start()
-        pl.semaphore_wait(
-            barrier,
-            jnp.where(r > 0, 1, 0) + jnp.where(r < n - 1, 1, 0)
-            + jnp.where(inner, 2, 0) + t,
-        )
+        greetings = jnp.where(r > 0, 1, 0) + jnp.where(inner, 2, 0) + t
+
+        @pl.when(greetings > 0)
+        def _():
+            pl.semaphore_wait(barrier, greetings)
+
+        @pl.when(has_next[1])
+        def _():
+            pl.semaphore_signal(answer, inc=1, device_id=ahead[1])
 
         @pl.when(inner)
         def _():
@@ -100,10 +106,17 @@
         def z_copy(p, way, k, j, src, dst):
             return remote(src, dst, zs.at[way], zr.at[p, way, k, j], ahead[way])
 
-        def send_own(p, way, pieces=range(chunks)):
-            for j in pieces:
+        def send_own(p, way):
+            for j in range(chunks):
                 block = w_all.at[p, r, rows_at(j), :]
                 z_copy(p, way, 0, j, block, block).start()
+
+        def send_part(way, low, high):
+            for j in range(chunks):
+                a, b = max(low, j * crow), min(high, (j + 1) * crow)
+                if a < b:
+                    block = w_all.at[0, r, a:b, :]
+                    z_copy(0, way, 0, j, block, block).start()
 
         def first_rows(q, count):
             return rows_all.at[q, pl.ds(0, count * tok), :]
@@ -142,16 +155,20 @@
             for way in range(2):
                 @pl.when(has_next[way])
                 def _(way=way):
-                    send_own(0, way, range(1, chunks))
+                    send_part(way, lead, shard)
 
                 @pl.when(depth[way] == 0)
                 def _(way=way):
                     send_own(1, way)
 
-        for way in range(2):
-            @pl.when(has_next[way])
-            def _(way=way):
-                send_own(0, way, range(1))
+        @pl.when(has_next[1])
+        def _():
+            send_part(1, 0, lead)
+
+        @pl.when(has_next[0])
+        def _():
+            pl.semaphore_wait(answer, 1)
+            send_part(0, 0, lead)
 
         loads[1].wait()
 
@@ -161,12 +178,13 @@
 
         spread_start(0)
         loads[2].wait()
+        loads[5].wait()
 
         @pl.when(t == 0)
         def _():
             rest_of_first_sends()
 
-        for load in loads[3:]:
+        for load in loads[3:5]:
             load.wait()
         tile = 2 * tok
 
@@ -364,7 +382,8 @@
     pl.run_scoped(
         all_but_last_step,
         dma((2, 2, n, chunks)), dma((2,)), dma((2, 2)), dma((2,)), dma((2,)),
-        dma(()), dma((n,)), dma((5,)), pltpu.SemaphoreType.REGULAR,
+        dma(()), dma((n,)), dma((6,)), pltpu.SemaphoreType.REGULAR,
+        pltpu.SemaphoreType.REGULAR,
     )
 
     def last(j, _):

time: 187 us -> 187 us (level); the launches traced: 184 us -> 186 us
  Pallas kernels: 184 us -> 186 us
    pallas_call x1, Pallas kernels: 181 us -> 183 us  [on_device(): pl.pallas_call(functools.partial(kernel, n, n_fs, chunks, factor), out_sh...]
where the time goes in v7:
time: 187 us; the launch traced here: 186 us
  Pallas kernels  186 us (99%)
    pallas_call x1, Pallas kernels, on_device(): pl.pallas_call(functools.partial(kernel, n, n_fs, chunks, factor), out_sh...  183 us

profile of v7, /device:TPU:0, one launch (start us, length us, event | category | flops | bytes accessed | tf_op | source)
XLA Modules:
  0.0 186.3 jit_solution(8186495816285654184)
XLA Ops:
  0.6 183.5 %shard_map.76 = (bf16[128,2048]{1,0:T(8,128)(2,1)S(1)}, f32[512,1024]{1,0:T(8,128)S(1)}, f32[512,1024]{1,0:T(8,128)S(1)}) custom-call(bf16[128,2048]{1,0:T(8,128)(2,1)} %x_ref.1, bf16[128,2048]{1,0:T(8,128)(2,1)} %og_ref.1, bf16[1024,1024]{1,0:T(8,128)(2,1)} %pre_ref.1, bf16[512,1024]{1,0:T(8,128)(2,1)} %wu_ref.1, bf16[512,1024]{1,0:T(8,128)(2,1)} %wd_ref.1), custom_call_target="tpu_custom_call" | custom-call | tf_op jit(solution)/shard_map/pallas_call | solution.py:430
  184.1 2.2 %shard_map.77 = (bf16[128,2048]{1,0:T(8,128)(2,1)}, f32[512,1024]{1,0:T(8,128)}, f32[512,1024]{1,0:T(8,128)}) custom-call(bf16[128,2048]{1,0:T(8,128)(2,1)S(1)} %get-tuple-element.6.refs_0_, f32[512,1024]{1,0:T(8,128)S(1)} %get-tuple-element.7.refs_1_, f32[512,1024]{1,0:T(8,128)S(1)} %get-tuple-element.8.refs_2_), custom_call_target="tpu_custom_call" | custom-call | tf_op jit(solution)/shard_map/pallas_call | solution.py:458

commit v8 on v7

--- a/solution.py
+++ b/solution.py
@@ -391,6 +391,17 @@
             @pl.when(depth[way] > 0)
             def _(way=way):
                 z_final(way, r, j).wait_recv()
+
+        @pl.when((depth[0] > 0) & (depth[1] > 0))
+        def _():
+            gu_ref[rows_at(j), :] += (
+                rs[1, 0, r, rows_at(j), :].astype(F32)
+                + rs[1, 1, r, rows_at(j), :].astype(F32)
+            )
+
+        for way in range(2):
+            @pl.when((depth[way] > 0) & (depth[1 - way] == 0))
+            def _(way=way):
                 gu_ref[rows_at(j), :] += rs[1, way, r, rows_at(j), :].astype(F32)
         return 0
 
@@ -413,8 +424,8 @@
     copies = [
         pltpu.make_async_copy(refs[i], refs[3 + i], refs[6].at[i]) for i in range(3)
     ]
-    for copy in copies:
-        copy.start()
+    for i, copy in ((2, copies[2]), (1, copies[1]), (0, copies[0])):
+        copy.start(priority=i % 2)
     for copy in copies:
         copy.wait()
 

time: 187 us -> 187 us (level)
  no operation moved by 1% of the time
where the time goes in v8:
time: 187 us; the launch traced here: 186 us
  Pallas kernels  186 us (99%)
    pallas_call x1, Pallas kernels, on_device(): pl.pallas_call(functools.partial(kernel, n, n_fs, chunks, factor), out_sh...  183 us

profile of v8, /device:TPU:0, one launch (start us, length us, event | category | flops | bytes accessed | tf_op | source)
XLA Modules:
  0.0 186.3 jit_solution(10274490676067708714)
XLA Ops:
  0.6 183.5 %shard_map.76 = (bf16[128,2048]{1,0:T(8,128)(2,1)S(1)}, f32[512,1024]{1,0:T(8,128)S(1)}, f32[512,1024]{1,0:T(8,128)S(1)}) custom-call(bf16[128,2048]{1,0:T(8,128)(2,1)} %x_ref.1, bf16[128,2048]{1,0:T(8,128)(2,1)} %og_ref.1, bf16[1024,1024]{1,0:T(8,128)(2,1)} %pre_ref.1, bf16[512,1024]{1,0:T(8,128)(2,1)} %wu_ref.1, bf16[512,1024]{1,0:T(8,128)(2,1)} %wd_ref.1), custom_call_target="tpu_custom_call" | custom-call | tf_op jit(solution)/shard_map/pallas_call | solution.py:441
  184.1 2.2 %shard_map.77 = (bf16[128,2048]{1,0:T(8,128)(2,1)}, f32[512,1024]{1,0:T(8,128)}, f32[512,1024]{1,0:T(8,128)}) custom-call(bf16[128,2048]{1,0:T(8,128)(2,1)S(1)} %get-tuple-element.6.refs_0_, f32[512,1024]{1,0:T(8,128)S(1)} %get-tuple-element.7.refs_1_, f32[512,1024]{1,0:T(8,128)S(1)} %get-tuple-element.8.refs_2_), custom_call_target="tpu_custom_call" | custom-call | tf_op jit(solution)/shard_map/pallas_call | solution.py:469

commit v9 on v7

--- a/solution.py
+++ b/solution.py
@@ -423,7 +423,7 @@
     tok, d_model = inputs.shape
     group, cols = pre_act.shape
     shard = w_up.shape[0]
-    chunks = max(1, shard // 256)
+    chunks = max(1, shard // 128)
     factor = float(group * n) ** -0.5
     dma = pltpu.SemaphoreType.DMA
     vmem = pl.BlockSpec(memory_space=pltpu.VMEM)

time: 187 us -> 187 us (level)
  no operation moved by 1% of the time
where the time goes in v9:
time: 187 us; the launch traced here: 186 us
  Pallas kernels  185 us (99%)
    pallas_call x1, Pallas kernels, on_device(): pl.pallas_call(functools.partial(kernel, n, n_fs, chunks, factor), out_sh...  183 us

profile of v9, /device:TPU:0, one launch (start us, length us, event | category | flops | bytes accessed | tf_op | source)
XLA Modules:
  0.0 185.6 jit_solution(5723504699766176371)
XLA Ops:
  0.6 182.8 %shard_map.76 = (bf16[128,2048]{1,0:T(8,128)(2,1)S(1)}, f32[512,1024]{1,0:T(8,128)S(1)}, f32[512,1024]{1,0:T(8,128)S(1)}) custom-call(bf16[128,2048]{1,0:T(8,128)(2,1)} %x_ref.1, bf16[128,2048]{1,0:T(8,128)(2,1)} %og_ref.1, bf16[1024,1024]{1,0:T(8,128)(2,1)} %pre_ref.1, bf16[512,1024]{1,0:T(8,128)(2,1)} %wu_ref.1, bf16[512,1024]{1,0:T(8,128)(2,1)} %wd_ref.1), custom_call_target="tpu_custom_call" | custom-call | tf_op jit(solution)/shard_map/pallas_call | solution.py:430
  183.4 2.2 %shard_map.77 = (bf16[128,2048]{1,0:T(8,128)(2,1)}, f32[512,1024]{1,0:T(8,128)}, f32[512,1024]{1,0:T(8,128)}) custom-call(bf16[128,2048]{1,0:T(8,128)(2,1)S(1)} %get-tuple-element.6.refs_0_, f32[512,1024]{1,0:T(8,128)S(1)} %get-tuple-element.7.refs_1_, f32[512,1024]{1,0:T(8,128)S(1)} %get-tuple-element.8.refs_2_), custom_call_target="tpu_custom_call" | custom-call | tf_op jit(solution)/shard_map/pallas_call | solution.py:458
